TPU v7x, 1024 devices: a 2x16x16 block of a 4x16x16 slice. The times are simulated.
1024 devices in a mesh: grp: 2 (over x), ep: 16 (over z), tp: 32 (over y, core).
Axes of the slice: x: 2, y: 16, z: 16, core: 2. Of those that a mesh axis runs over, the one named last changes fastest.
The devices are a block of a 4x16x16 slice.
Arguments:
- tokens: bfloat16 [2048, 2048], P(('grp', 'ep')), parts along dimension 0, may hold values from -6 to 6
- norm_gain: float32 [2048], replicated, may hold values from 0.1 to 1.9
- routes: int32 [2048, 8], P(('grp', 'ep')), parts along dimension 0, may hold values from 0 to 255, all different within a row; in each aligned block of 64 rows (0 to 63, 64 to 127, ...) at most 4 rows name the same one
- route_weight: float32 [2048, 8], P(('grp', 'ep')), parts along dimension 0, may hold values from 0.05 to 1
- gate_proj: bfloat16 [512, 2048, 256], P(('ep', 'tp')), may hold values from -0.125 to 0.125
- up_proj: bfloat16 [512, 2048, 256], P(('ep', 'tp')), may hold values from -0.125 to 0.125
- down_proj: bfloat16 [512, 256, 2048], P(('ep', 'tp')), may hold values from -0.25 to 0.25
- shared_gate: bfloat16 [2048, 512], P(None, 'tp'), may hold values from -0.125 to 0.125
- shared_up: bfloat16 [2048, 512], P(None, 'tp'), may hold values from -0.125 to 0.125
- shared_down: bfloat16 [512, 2048], P('tp'), may hold values from -0.25 to 0.25
Outputs:
- mixed: bfloat16 [2048, 2048], P(('grp', 'ep'), 'tp'), parts along dimension 0
There are 2 independent parts, one for each index of `grp`. A program takes and returns all parts, laid end to end along the dimension named above; an argument that names none is the same for every part. Nothing has to cross between parts.
Inputs may be any that keep to these rules, and one draw needn't show every extreme that they name: `routes`: each row names 8 different experts. Among the 64 rows of one ep index no expert is named by more than 4 rows, a bound that some block reaches of them.
All inputs are finite; a program needn't handle non-finite values.
Results may differ from a plain program's by a relative error of at most 0.0064.
Values may be sent and summed in bfloat16 or wider, within the bound.
No kernel may reach another device: no remote copies, remote signals or barrier semaphores. Data moves between devices by JAX's collectives and lax.ppermute only.
A program may use at most 32 MiB of HBM per device.

v0:
```python
import jax
import jax.numpy as jnp
from jax import lax
from jax.sharding import PartitionSpec as P

EXPERT_SHARDS = 2


eps = 1e-06
routed_scale = 2.5


def in_blocks(shard, dim, length):
    dims = shard.shape
    tiles = shard.reshape(*dims[:dim], length, dims[dim] // length, *dims[dim + 1 :])
    return jnp.moveaxis(tiles, dim, 0)


def sum_at_owner(shard, axis, dim):
    length = lax.axis_size(axis)
    tiles = lax.all_to_all(in_blocks(shard, dim, length), axis, 0, 0, tiled=True)
    return jnp.sum(tiles, axis=0)


def norm_rows(tokens, norm_gain):
    values = tokens.astype(jnp.float32)
    scaled = values * lax.rsqrt(jnp.mean(values * values, axis=-1, keepdims=True) + eps)
    return (scaled * norm_gain).astype(jnp.bfloat16)


def expert_apply(row_block, gate_half, up_half, down_half):
    gate_part = jnp.dot(row_block, gate_half, preferred_element_type=jnp.float32)
    upper = jnp.dot(row_block, up_half, preferred_element_type=jnp.float32)
    active = (jax.nn.silu(gate_part) * upper).astype(jnp.bfloat16)
    return jnp.dot(active, down_half, preferred_element_type=jnp.float32)


def slot_table(hit_table, capacity):
    counts = jnp.cumsum(hit_table.astype(jnp.int32), axis=1) - 1
    slots = jnp.arange(capacity, dtype=jnp.int32)
    return hit_table[:, None, :] & (counts[:, None, :] == slots[None, :, None])


def per_device(
    tokens,
    norm_gain,
    routes,
    route_weight,
    gate_proj,
    up_proj,
    down_proj,
    shared_gate,
    shared_up,
    shared_down,
):
    ep_count = lax.axis_size("ep")
    tp_count = lax.axis_size("tp")
    per_block = tp_count // EXPERT_SHARDS
    experts = ep_count * per_block
    tok_rows, top_count = routes.shape
    capacity = min(tok_rows, max(2, 2 * tok_rows * top_count // experts))
    column = lax.axis_index("tp") // EXPERT_SHARDS
    normed = norm_rows(tokens, norm_gain)
    mixing = route_weight / jnp.sum(route_weight, axis=1, keepdims=True) * routed_scale
    targets = jnp.arange(ep_count, dtype=jnp.int32) * per_block + column
    matches = routes[:, :, None] == targets[None, None, :]
    sent_hits = jnp.any(matches, axis=1).T
    weights_out = jnp.sum(jnp.where(matches, mixing[:, :, None], 0.0), axis=1).T
    sending = slot_table(sent_hits, capacity)
    gate_half = gate_proj[0]
    up_half = up_proj[0]
    down_half = down_proj[0]
    outgoing = jnp.einsum(
        "kct,td->kcd", sending.astype(jnp.bfloat16), normed, preferred_element_type=jnp.float32
    ).astype(jnp.bfloat16)
    arrived = lax.all_to_all(outgoing, "ep", split_axis=0, concat_axis=0, tiled=True)
    sources, slot_count, feature_width = arrived.shape
    produced = expert_apply(
        arrived.reshape(sources * slot_count, feature_width), gate_half, up_half, down_half
    )
    produced = produced.reshape(sources, slot_count, -1)
    returned = lax.all_to_all(produced, "ep", split_axis=0, concat_axis=0, tiled=True)
    weighting = sending.astype(jnp.float32) * weights_out[:, None, :]
    routed = jnp.einsum("kct,kcd->td", weighting, returned, precision=lax.Precision.HIGHEST)
    shared_term = expert_apply(normed, shared_gate, shared_up, shared_down)
    return sum_at_owner(routed + shared_term, "tp", 1).astype(jnp.bfloat16)


def solution(mesh):
    in_specs = (
        P(("grp", "ep"), None),
        P(),
        P(("grp", "ep"), None),
        P(("grp", "ep"), None),
        P(("ep", "tp"), None, None),
        P(("ep", "tp"), None, None),
        P(("ep", "tp"), None, None),
        P(None, "tp"),
        P(None, "tp"),
        P("tp", None),
    )
    out_specs = P(("grp", "ep"), "tp")
    return jax.shard_map(
        per_device, mesh=mesh, in_specs=in_specs, out_specs=out_specs, check_vma=False
    )
```

profile of v0, /device:TPU:6, one launch (start us, length us, event | category | flops | bytes accessed | tf_op | source)
XLA Modules:
  0.0 196.8 jit_solution(12877331337403865387)
XLA Ops:
  0.0 0.0 copy-start
  0.0 0.0 copy-start.1
  0.0 0.9 compare_reduce_fusion
  0.9 0.2 reduce_window_sum.11
  1.1 0.0 copy-start.6
  1.1 1.1 fusion.7
  2.3 0.0 copy-done.1
  2.3 0.0 copy-done.6
  2.3 0.0 copy-start.2
  2.3 0.3 convolution_convert_fusion
  2.6 0.2 copy.23
  2.8 101.0 %all_to_all.15 = bf16[16,4,2048]{2,1,0:T(4,128)(2,1)S(1)} all-to-all(bf16[16,4,2048]{2,1,0:T(4,128)(2,1)S(1)} %copy.23), channel_id=1, replica_groups=mesh['grp'=2,'ep'=16,'tp'=32] {'ep'}, dimensions={0} | all-to-all | bytes 524288 | tf_op jit(solution)/shard_map/all_to_all | solution.py:76
  103.8 0.1 reshape.34
  103.9 0.0 copy-done.2
  103.9 0.0 copy-start.3
  103.9 0.3 fusion.5
  104.2 0.9 copy-done.3
  105.1 0.3 fusion
  105.4 0.0 copy-done
  105.5 0.3 fusion.2
  105.8 1.1 copy.25
  106.9 0.0 copy-start.7
  106.9 0.0 copy-start.9
  106.9 6.2 %all-to-all-start.1 = ((f32[16,4,2048]{2,1,0:T(4,128)}), f32[16,4,2048]{2,1,0:T(4,128)S(1)}, u32[]{:S(2)}, u32[]{:S(2)}) async-start(f32[16,4,2048]{2,1,0:T(4,128)} %copy.25), calls=%async_computation.1 | async-start | bytes 1048576 | tf_op jit(solution)/shard_map/all_to_all | solution.py:82
  113.1 0.0 copy-done.7
  113.2 0.0 copy-start.8
  113.2 0.7 copy-done.8
  113.9 0.1 fusion.12
  113.9 0.0 copy-done.9
  114.0 0.2 fusion.34
  114.2 27.8 %all-to-all-done.1 = f32[16,4,2048]{2,1,0:T(4,128)S(1)} async-done(((f32[16,4,2048]{2,1,0:T(4,128)}), f32[16,4,2048]{2,1,0:T(4,128)S(1)}, u32[]{:S(2)}, u32[]{:S(2)}) %all-to-all-start.1) | async-done | bytes 524320 | tf_op jit(solution)/shard_map/all_to_all | solution.py:82
  142.0 0.0 copy-start.4
  142.0 0.0 copy-start.5
  142.0 0.9 convolution_bitcast_fusion
  142.9 0.0 copy-done.4
  142.9 0.0 copy-done.5
  142.9 0.6 convolution_add_fusion
  143.5 0.4 reshape.35
  143.9 0.6 copy.33
  144.6 0.7 reshape.39
  145.2 48.1 %all_to_all.16 = f32[32,1,4096]{2,1,0:T(1,128)S(1)} all-to-all(f32[32,1,4096]{2,1,0:T(1,128)S(1)} %reshape.39), channel_id=1, replica_groups=mesh['grp'=2,'ep'=16,'tp'=32] {'tp'}, dimensions={0} | all-to-all | bytes 1048576 | tf_op jit(solution)/shard_map/all_to_all | solution.py:21
  193.3 0.5 broadcast.52
  193.8 1.9 reduce
  195.7 0.4 reshape.40
  196.1 0.7 reduce_sum.39
  (7 shorter events, 0.1 us)
Async XLA Ops:
  0.0 105.4 %copy-start = (bf16[1,256,2048]{2,1,0:T(8,128)(2,1)S(1)}, bf16[1,256,2048]{2,1,0:T(8,128)(2,1)}, u32[]{:S(2)}) copy-start(bf16[1,256,2048]{2,1,0:T(8,128)(2,1)} %param.16) | copy-start | bytes 3145732
  0.0 2.3 %copy-start.1 = (bf16[64,2048]{1,0:T(8,128)(2,1)S(1)}, bf16[64,2048]{1,0:T(8,128)(2,1)}, u32[]{:S(2)}) copy-start(bf16[64,2048]{1,0:T(8,128)(2,1)} %param.10) | copy-start | bytes 786436
  1.1 1.1 copy-start.6
  2.3 101.6 %copy-start.2 = (bf16[1,2048,256]{2,1,0:T(8,128)(2,1)S(1)}, bf16[1,2048,256]{2,1,0:T(8,128)(2,1)}, u32[]{:S(2)}) copy-start(bf16[1,2048,256]{2,1,0:T(8,128)(2,1)} %param.14) | copy-start | bytes 3145732
  103.9 1.2 copy-start.3
  106.9 6.3 %copy-start.7 = (f32[64,8]{0,1:T(8,128)S(1)}, f32[64,8]{0,1:T(8,128)}, u32[]{:S(2)}) copy-start(f32[64,8]{0,1:T(8,128)} %param.13) | copy-start | bytes 6148
  106.9 7.1 %copy-start.9 = (bf16[2048,16]{0,1:T(8,128)(2,1)S(1)}, bf16[2048,16]{0,1:T(8,128)(2,1)}, u32[]{:S(2)}) copy-start(bf16[2048,16]{0,1:T(8,128)(2,1)} %param.17) | copy-start | bytes 196612
  106.9 35.1 %all-to-all-start.1 = ((f32[16,4,2048]{2,1,0:T(4,128)}), f32[16,4,2048]{2,1,0:T(4,128)S(1)}, u32[]{:S(2)}, u32[]{:S(2)}) async-start(f32[16,4,2048]{2,1,0:T(4,128)} %copy.25), calls=%async_computation.1 | async-start | bytes 1048576 | tf_op jit(solution)/shard_map/all_to_all | solution.py:82
  113.2 0.7 copy-start.8
  142.0 0.9 copy-start.4
  142.0 0.9 copy-start.5
where the time goes:
time: 198 us; the launch traced here: 197 us
  blocking collectives  149 us (75%)
  waiting for transfers between devices  27.8 us (14%)
  starting transfers between devices  6.24 us (3%)
  local copies, waits for them, and re-layouts  5.63 us (3%)
  other arithmetic  4.93 us (2%)
  matrix products  2.92 us (1%)
    all_to_all x1, blocking collectives, per_device(): lax.all_to_all(outgoing, 'ep', split_axis=0, concat_axis=0, tiled=True)  101 us
    all_to_all x1, blocking collectives, sum_at_owner(): lax.all_to_all(in_blocks(shard, dim, length), axis, 0, 0, tiled=True)  48.1 us
    all_to_all x1, waiting for transfers between devices, per_device(): lax.all_to_all(produced, 'ep', split_axis=0, concat_axis=0, tiled=True)  27.8 us
    all_to_all x1, starting transfers between devices, per_device(): lax.all_to_all(produced, 'ep', split_axis=0, concat_axis=0, tiled=True)  6.24 us
  transfers between devices with their start and end apart: 1, of which 1 were waited for; matrix products, arithmetic and copies ran while one was open for 0% of the time, Pallas kernels for 0%

commit v1 on v0

v1 whole, which is shorter than its diff:
```python
import functools

import jax
import jax.numpy as jnp
from jax import lax
from jax.experimental import pallas as pl
from jax.experimental.pallas import tpu as pltpu
from jax.sharding import PartitionSpec as P

EXPERT_SHARDS = 2
LANES = 128
HALF = LANES // 2

eps = 1e-06
routed_scale = 2.5

VMEM = pl.BlockSpec(memory_space=pltpu.VMEM)
SMEM = pl.BlockSpec(memory_space=pltpu.SMEM)


def call(kernel, outs, in_specs, name, flops, mib=16):
    return pl.pallas_call(
        kernel,
        out_shape=outs,
        in_specs=in_specs,
        out_specs=jax.tree.map(lambda _: VMEM, outs),
        compiler_params=pltpu.CompilerParams(vmem_limit_bytes=mib << 20),
        cost_estimate=pl.CostEstimate(flops=flops, bytes_accessed=1 << 20, transcendentals=0),
        name=name,
    )


def hits_of(routes_t, targets):
    hit = routes_t[0:1, :] == targets
    for j in range(1, routes_t.shape[0]):
        hit = hit | (routes_t[j : j + 1, :] == targets)
    return hit


def slots_of(hit):
    tokens = hit.shape[1]
    before = lax.broadcasted_iota(jnp.int32, (tokens, tokens), 0)
    after = lax.broadcasted_iota(jnp.int32, (tokens, tokens), 1)
    lower = jnp.where(before <= after, 1.0, 0.0).astype(jnp.bfloat16)
    ones = jnp.where(hit, 1.0, 0.0).astype(jnp.bfloat16)
    return jnp.dot(ones, lower, preferred_element_type=jnp.float32)


def row_parts(rows, tokens, capacity):
    row = lax.broadcasted_iota(jnp.int32, (rows, tokens), 0)
    peer = row // (2 * capacity)
    half = (row // capacity) % 2
    slot = row % capacity
    return peer, half, slot


def select_rows(col_ref, routes_t, rows, tokens, capacity, per_block):
    peer, half, slot = row_parts(rows, tokens, capacity)
    hit = hits_of(routes_t, peer * per_block + col_ref[0])
    counts = slots_of(hit)
    return hit & (counts == (slot + 1).astype(jnp.float32)), half


def dispatch_kernel(capacity, per_block, col_ref, routes_ref, tokens_ref, gain_ref, out_ref, normed_ref):
    values = tokens_ref[...].astype(jnp.float32)
    width = values.shape[1]
    scale = lax.rsqrt(jnp.sum(values * values, axis=-1, keepdims=True) * (1.0 / width) + eps)
    normed = (values * scale * gain_ref[...]).astype(jnp.bfloat16)
    normed_ref[...] = normed
    tokens = values.shape[0]
    rows = out_ref.shape[0]
    chosen, half = select_rows(col_ref, routes_ref[...], rows, tokens, capacity, per_block)
    first = jnp.where(chosen & (half == 0), 1.0, 0.0).astype(jnp.bfloat16)
    second = jnp.where(chosen & (half == 1), 1.0, 0.0).astype(jnp.bfloat16)
    low, high = normed[:, : width // 2], normed[:, width // 2 :]
    out = jnp.dot(first, low, preferred_element_type=jnp.float32)
    out = out + jnp.dot(second, high, preferred_element_type=jnp.float32)
    out_ref[...] = out.astype(jnp.bfloat16)


def silu_times(gate, up):
    return (gate / (1.0 + jnp.exp(-gate)) * up).astype(jnp.bfloat16)


def split_by_core(core, full):
    rows, width = full.shape
    lane = lax.broadcasted_iota(jnp.int32, (rows, LANES), 1)
    low = lane < HALF
    mine, theirs = [], []
    for j in range(0, width // LANES, 2):
        even = full[:, j * LANES : (j + 1) * LANES]
        odd = full[:, (j + 1) * LANES : (j + 2) * LANES]
        firsts = jnp.where(low, even, pltpu.roll(odd, HALF, 1))
        lasts = jnp.where(low, pltpu.roll(even, HALF, 1), odd)
        mine.append(jnp.where(core == 0, firsts, lasts))
        theirs.append(jnp.where(core == 0, lasts, firsts))
    return jnp.concatenate(mine, axis=1), jnp.concatenate(theirs, axis=1)


def side_kernel(
    capacity, per_block, col_ref, routes_ref, weight_ref, normed_ref, gate_ref, up_ref, down_ref,
    weights_ref, mine_ref, theirs_ref,
):
    routes_t = routes_ref[...]
    weight_t = weight_ref[...]
    mixing = weight_t / jnp.sum(weight_t, axis=0, keepdims=True) * routed_scale
    choices, tokens = routes_t.shape
    rows = weights_ref.shape[1]
    chosen, half = select_rows(col_ref, routes_t, rows, tokens, capacity, per_block)
    peer, _, _ = row_parts(rows, tokens, capacity)
    target = peer * per_block + col_ref[0]
    scale = jnp.zeros((rows, tokens), jnp.float32)
    for j in range(choices):
        scale = scale + jnp.where(routes_t[j : j + 1, :] == target, mixing[j : j + 1, :], 0.0)
    for h in range(2):
        table = jnp.where(chosen & (half == h), scale, 0.0)
        top = table.astype(jnp.bfloat16)
        rest = (table - top.astype(jnp.float32)).astype(jnp.bfloat16)
        weights_ref[h] = jnp.concatenate([top, rest], axis=1)
    normed = normed_ref[...]
    contract = (((1,), (1,)), ((), ()))
    gate = lax.dot_general(normed, gate_ref[...], contract, preferred_element_type=jnp.float32)
    up = lax.dot_general(normed, up_ref[...], contract, preferred_element_type=jnp.float32)
    active = silu_times(gate, up)
    full = jnp.dot(active, down_ref[...], preferred_element_type=jnp.float32)
    mine, theirs = split_by_core(col_ref[1], full)
    mine_ref[...] = mine
    theirs_ref[...] = theirs.astype(jnp.bfloat16)


def expert_kernel(
    capacity, col_ref, rows_ref, gate_ref, up_ref, down_ref, shared_ref, mine_ref, theirs_ref
):
    x = rows_ref[...]
    rows, depth = x.shape

    def product(weights):
        low = jnp.dot(x, weights[:depth], preferred_element_type=jnp.float32)
        high = jnp.dot(x, weights[depth:], preferred_element_type=jnp.float32)
        return low + pltpu.roll(high, rows - capacity, 0)

    active = silu_times(product(gate_ref[0]), product(up_ref[0]))
    full = jnp.dot(active, down_ref[0], preferred_element_type=jnp.float32)
    mine, theirs = split_by_core(col_ref[1], full)
    half = mine.shape[1] // 2
    row = lax.broadcasted_iota(jnp.int32, (rows, half), 0)
    first = (row // capacity) % 2 == 0

    def fold(v):
        return jnp.where(first, v[:, :half], pltpu.roll(v[:, half:], capacity, 0))

    mine_ref[...] = fold(mine)
    theirs_ref[:rows] = fold(theirs).astype(jnp.bfloat16)
    shared = shared_ref[...]
    tokens = shared.shape[0]
    theirs_ref[rows : rows + tokens] = shared[:, :half]
    theirs_ref[rows + tokens :] = shared[:, half:]


def pair_kernel(mine_ref, theirs_ref, out_ref):
    rows = mine_ref.shape[0]
    out_ref[...] = (mine_ref[...] + theirs_ref[:rows].astype(jnp.float32)).astype(jnp.bfloat16)


def combine_kernel(returned_ref, weights_ref, shared_ref, theirs_ref, out_ref):
    returned = returned_ref[...]
    rows, half = returned.shape
    tokens = shared_ref.shape[0]
    contract = (((0,), (0,)), ((), ()))
    halves = []
    for h in range(2):
        both = lax.dot_general(weights_ref[h], returned, contract, preferred_element_type=jnp.float32)
        routed = both[:tokens] + both[tokens:]
        first = rows + h * tokens
        shared = shared_ref[:, h * half : (h + 1) * half] + theirs_ref[first : first + tokens].astype(jnp.float32)
        halves.append(routed + shared)
    total = jnp.concatenate(halves, axis=1)
    part = tokens // 2
    low = lax.broadcasted_iota(jnp.int32, (part, LANES), 1) < HALF
    for j in range(total.shape[1] // LANES):
        tile = total[:, j * LANES : (j + 1) * LANES]
        turned = pltpu.roll(tile, HALF, 1)
        even = jnp.where(low, tile[:part], turned[part:])
        odd = jnp.where(low, turned[:part], tile[part:])
        out_ref[2 * j * part : (2 * j + 1) * part] = even.astype(jnp.bfloat16)
        out_ref[(2 * j + 1) * part : (2 * j + 2) * part] = odd.astype(jnp.bfloat16)


def final_kernel(count, parts_ref, out_ref):
    part = parts_ref.shape[0] // count
    total = parts_ref[:part].astype(jnp.float32)
    for i in range(1, count):
        total = total + parts_ref[i * part : (i + 1) * part].astype(jnp.float32)
    turned = pltpu.roll(total, HALF, 1)
    out_ref[:part] = total[:, :HALF].astype(jnp.bfloat16)
    out_ref[part:] = turned[:, :HALF].astype(jnp.bfloat16)


def per_device(
    tokens,
    norm_gain,
    routes,
    route_weight,
    gate_proj,
    up_proj,
    down_proj,
    shared_gate,
    shared_up,
    shared_down,
):
    ep_count = lax.axis_size("ep")
    tp_count = lax.axis_size("tp")
    per_block = tp_count // EXPERT_SHARDS
    experts = ep_count * per_block
    tok_rows, top_count = routes.shape
    width = tokens.shape[1]
    capacity = min(tok_rows, max(2, 2 * tok_rows * top_count // experts))
    rows = ep_count * 2 * capacity
    tp = lax.axis_index("tp")
    place = jnp.stack([tp // EXPERT_SHARDS, tp % EXPERT_SHARDS]).astype(jnp.int32)
    routes_t, weight_t = routes.T, route_weight.T
    f32, bf16 = jnp.float32, jnp.bfloat16
    shape = jax.ShapeDtypeStruct

    with jax.named_scope("dispatch"):
        outgoing, normed = call(
            functools.partial(dispatch_kernel, capacity, per_block),
            (shape((rows, width // 2), bf16), shape((tok_rows, width), bf16)),
            [SMEM, VMEM, VMEM, VMEM],
            "dispatch",
            1 << 27,
        )(place, routes_t, tokens, norm_gain.reshape(1, width))
        arrived = lax.all_to_all(
            outgoing.reshape(ep_count, 2 * capacity, width // 2), "ep", 0, 0, tiled=True
        )
    with jax.named_scope("side"):
        weights, shared_mine, shared_theirs = call(
            functools.partial(side_kernel, capacity, per_block),
            (
                shape((2, rows, 2 * tok_rows), bf16),
                shape((tok_rows, width // 2), f32),
                shape((tok_rows, width // 2), bf16),
            ),
            [SMEM] + [VMEM] * 6,
            "side",
            1 << 30,
        )(place, routes_t, weight_t, normed, shared_gate.T, shared_up.T, shared_down)
    with jax.named_scope("experts"):
        mine, theirs = call(
            functools.partial(expert_kernel, capacity),
            (shape((rows, width // 4), f32), shape((rows + 2 * tok_rows, width // 4), bf16)),
            [SMEM] + [VMEM] * 5,
            "experts",
            1 << 28,
        )(place, arrived.reshape(rows, width // 2), gate_proj, up_proj, down_proj, shared_theirs)
    with jax.named_scope("pair"):
        theirs = lax.ppermute(theirs, "tp", [(i, i ^ 1) for i in range(tp_count)])
        produced = call(pair_kernel, shape((rows, width // 4), bf16), [VMEM] * 2, "pair", 1 << 20)(mine, theirs)
    with jax.named_scope("back"):
        returned = lax.all_to_all(
            produced.reshape(ep_count, 2 * capacity, width // 4), "ep", 0, 0, tiled=True
        )
    with jax.named_scope("combine"):
        sums = call(
            combine_kernel,
            shape((per_block * tok_rows // 2, LANES), bf16),
            [VMEM] * 4,
            "combine",
            1 << 26,
        )(returned.reshape(rows, width // 4), weights, shared_mine, theirs)
        groups = [list(range(core, tp_count, EXPERT_SHARDS)) for core in range(EXPERT_SHARDS)]
        parts = lax.all_to_all(
            sums.reshape(per_block, tok_rows // 2, LANES), "tp", 0, 0, tiled=True, axis_index_groups=groups
        )
    with jax.named_scope("final"):
        return call(
            functools.partial(final_kernel, per_block),
            shape((tok_rows, width // tp_count), bf16),
            [VMEM],
            "final",
            1 << 20,
        )(parts.reshape(per_block * tok_rows // 2, LANES))


def solution(mesh):
    in_specs = (
        P(("grp", "ep"), None),
        P(),
        P(("grp", "ep"), None),
        P(("grp", "ep"), None),
        P(("ep", "tp"), None, None),
        P(("ep", "tp"), None, None),
        P(("ep", "tp"), None, None),
        P(None, "tp"),
        P(None, "tp"),
        P("tp", None),
    )
    out_specs = P(("grp", "ep"), "tp")
    return jax.shard_map(
        per_device, mesh=mesh, in_specs=in_specs, out_specs=out_specs, check_vma=False
    )
```

time: 198 us -> 160 us (0.81)
  blocking collectives: 149 us -> 47.7 us
  starting transfers between devices: 6.24 us -> 85 us
  waiting for transfers between devices: 27.8 us -> 13 us
  Pallas kernels: 0 us -> 5.39 us
  other arithmetic: 4.93 us -> 0.07 us
  matrix products: 2.92 us -> 0 us
  local copies, waits for them, and re-layouts: 5.63 us -> 7.73 us
    all_to_all x2, blocking collectives: 149 us -> 47.7 us  [the longest x1 27.2 us: per_device(): lax.all_to_all(sums.reshape(per_block, tok_rows // 2, LANES), 'tp', 0, 0,...]
    all_to_all x1, starting transfers between devices: 6.24 us -> 83.1 us  [per_device(): lax.all_to_all(outgoing.reshape(ep_count, 2 * capacity, width // 2), 'ep'...]
    all_to_all x1, waiting for transfers between devices: 27.8 us -> 11.4 us  [per_device(): lax.all_to_all(outgoing.reshape(ep_count, 2 * capacity, width // 2), 'ep'...]
    pallas_call x0 -> x6, Pallas kernels: none -> 5.39 us  [the longest x1 1.68 us: per_device(): call(functools.partial(dispatch_kernel, capacity, per_block), (shape((row...]
    unnamed x22 -> x32, local copies, waits for them, and re-layouts: 2.68 us -> 7.73 us
    dot_general x7 -> x0, matrix products: 2.92 us -> none  [the longest x2 0.93 us: expert_apply(): return jnp.dot(active, down_half, preferred_element_type=jnp.float32)]
  transfers between devices with their start and end apart: 1 -> 2, of which waited for: 1 -> 2; matrix products, arithmetic and copies ran while one was open for 0% -> 0% of each run, Pallas kernels for 0% -> 1%
where the time goes in v1:
time: 160 us; the launch traced here: 159 us
  starting transfers between devices  85 us (53%)
  blocking collectives  47.7 us (30%)
  waiting for transfers between devices  13 us (8%)
  local copies, waits for them, and re-layouts  7.73 us (5%)
  Pallas kernels  5.39 us (3%)
    all_to_all x1, starting transfers between devices, per_device(): lax.all_to_all(outgoing.reshape(ep_count, 2 * capacity, width // 2), 'ep'...  83.1 us
    all_to_all x1, blocking collectives, per_device(): lax.all_to_all(sums.reshape(per_block, tok_rows // 2, LANES), 'tp', 0, 0,...  27.2 us
    all_to_all x1, blocking collectives, per_device(): lax.all_to_all(produced.reshape(ep_count, 2 * capacity, width // 4), 'ep'...  20.6 us
    all_to_all x1, waiting for transfers between devices, per_device(): lax.all_to_all(outgoing.reshape(ep_count, 2 * capacity, width // 2), 'ep'...  11.4 us
    unnamed x32, local copies, waits for them, and re-layouts  7.73 us
  transfers between devices with their start and end apart: 2, of which 2 were waited for; matrix products, arithmetic and copies ran while one was open for 0% of the time, Pallas kernels for 1%

profile of v1, /device:TPU:6, one launch (start us, length us, event | category | flops | bytes accessed | tf_op | source)
XLA Modules:
  0.0 159.0 jit_solution(7079964340036191148)
XLA Ops:
  0.0 0.0 copy-start.11
  0.0 0.0 copy-start.12
  0.0 0.1 pad_add_fusion.col_ref
  0.1 0.6 copy-done.11
  0.7 0.0 copy-done.12
  0.7 0.0 copy-start.7
  0.7 0.9 copy-done.7
  1.7 1.7 %dispatch.1 = (bf16[128,1024]{1,0:T(8,128)(2,1)}, bf16[64,2048]{1,0:T(8,128)(2,1)S(1)}) custom-call(s32[2]{0:T(128)S(1)} %pad_add_fusion.col_ref, s32[8,64]{1,0:T(8,128)S(1)} %bitcast.21, bf16[64,2048]{1,0:T(8,128)(2,1)S(1)} %copy-done.7, f32[1,2048]{1,0:T(1,128)S(1)} %bitcast.20), custom_call_target="tpu_custom_call" | custom-call | flops 134217728 | bytes 1048576 | tf_op jit(solution)/shard_map/dispatch/dispatch/pallas_call | solution.py:226
  3.3 0.0 copy-start.14
  3.3 0.7 copy-done.14
  4.0 83.1 %all-to-all-start = ((bf16[16,8,1024]{2,1,0:T(8,128)(2,1)}), bf16[16,8,1024]{2,1,0:T(8,128)(2,1)S(1)}, u32[]{:S(2)}, u32[]{:S(2)}) async-start(bf16[16,8,1024]{2,1,0:T(8,128)(2,1)} %bitcast.4), calls=%async_computation | async-start | bytes 524288 | tf_op jit(solution)/shard_map/dispatch/all_to_all | solution.py:233
  87.1 0.0 copy-start.13
  87.1 0.7 copy-done.13
  87.8 0.0 copy-start.8
  87.8 0.8 copy-done.8
  88.7 0.0 copy-start.9
  88.7 0.8 copy-done.9
  89.5 0.0 copy-start.10
  89.5 0.8 copy-done.10
  90.3 0.0 copy-start.15
  90.3 0.9 copy-done.15
  91.3 0.0 copy-start
  91.3 0.0 copy-start.1
  91.3 0.0 copy-start.2
  91.3 1.2 side.1
  92.5 0.0 copy-start.3
  92.5 0.7 copy-done.3
  93.2 0.0 copy-start.5
  93.2 0.6 copy-done.5
  93.8 11.4 %all-to-all-done = bf16[16,8,1024]{2,1,0:T(8,128)(2,1)S(1)} async-done(((bf16[16,8,1024]{2,1,0:T(8,128)(2,1)}), bf16[16,8,1024]{2,1,0:T(8,128)(2,1)S(1)}, u32[]{:S(2)}, u32[]{:S(2)}) %all-to-all-start) | async-done | bytes 262176 | tf_op jit(solution)/shard_map/dispatch/all_to_all | solution.py:233
  105.3 0.0 copy-done
  105.3 0.0 copy-done.1
  105.3 0.0 copy-done.2
  105.3 1.5 experts.1
  106.7 2.0 %collective-permute-start = (bf16[256,512]{1,0:T(8,128)(2,1)S(1)}, bf16[256,512]{1,0:T(8,128)(2,1)S(1)}, u32[]{:S(2)}, u32[]{:S(2)}) collective-permute-start(bf16[256,512]{1,0:T(8,128)(2,1)S(1)} %get-tuple-element.16), channel_id=1, source_target_pairs={{0,1},{1,0},{2,3},{3,2},{4,5},{5,4},{6,7},{7,6},{8,9},{9,8},{10,11... | collective-permute-start | bytes 786440 | tf_op jit(solution)/shard_map/pair/ppermute | solution.py:257
  108.7 1.5 collective-permute-done.theirs_ref
  110.2 0.0 copy-start.6
  110.2 0.0 copy-start.4
  110.2 20.6 %all_to_all.15 = bf16[16,8,512]{2,1,0:T(8,128)(2,1)S(1)} all-to-all(bf16[16,8,512]{2,1,0:T(8,128)(2,1)S(1)} %bitcast.14), channel_id=1, replica_groups=mesh['grp'=2,'ep'=16,'tp'=32] {'ep'}, dimensions={0} | all-to-all | bytes 262144 | tf_op jit(solution)/shard_map/back/all_to_all | solution.py:260
  130.8 0.0 copy-done.6
  130.8 0.0 copy-done.4
  130.8 0.3 combine.1
  131.1 27.2 %all_to_all.16 = bf16[16,32,128]{2,1,0:T(8,128)(2,1)S(1)} all-to-all(bf16[16,32,128]{2,1,0:T(8,128)(2,1)S(1)} %bitcast.17), channel_id=1, replica_groups={{0,2,4,6,8,10,12,14,16,18,20,22,24,26,28,30},{1,3,5,7,9,11,13,15,17,19,..., dimensions={0} | all-to-all | bytes 262144 | tf_op jit(solution)/shard_map/combine/all_to_all | solution.py:272
  158.3 0.7 final.1
  (1 shorter events, 0.0 us)
Async XLA Ops:
  0.0 0.7 copy-start.11
  0.0 0.7 copy-start.12
  0.7 0.9 copy-start.7
  3.3 0.7 copy-start.14
  4.0 101.2 %all-to-all-start = ((bf16[16,8,1024]{2,1,0:T(8,128)(2,1)}), bf16[16,8,1024]{2,1,0:T(8,128)(2,1)S(1)}, u32[]{:S(2)}, u32[]{:S(2)}) async-start(bf16[16,8,1024]{2,1,0:T(8,128)(2,1)} %bitcast.4), calls=%async_computation | async-start | bytes 524288 | tf_op jit(solution)/shard_map/dispatch/all_to_all | solution.py:233
  87.1 0.7 copy-start.13
  87.8 0.8 copy-start.8
  88.7 0.8 copy-start.9
  89.5 0.8 copy-start.10
  90.3 0.9 copy-start.15
  91.3 14.0 %copy-start = (bf16[1,2048,256]{2,1,0:T(8,128)(2,1)S(1)}, bf16[1,2048,256]{2,1,0:T(8,128)(2,1)}, u32[]{:S(2)}) copy-start(bf16[1,2048,256]{2,1,0:T(8,128)(2,1)} %gate_ref.1) | copy-start | bytes 3145732
  91.3 14.0 %copy-start.1 = (bf16[1,2048,256]{2,1,0:T(8,128)(2,1)S(1)}, bf16[1,2048,256]{2,1,0:T(8,128)(2,1)}, u32[]{:S(2)}) copy-start(bf16[1,2048,256]{2,1,0:T(8,128)(2,1)} %up_ref.1) | copy-start | bytes 3145732
  91.3 14.0 %copy-start.2 = (bf16[1,256,2048]{2,1,0:T(8,128)(2,1)S(1)}, bf16[1,256,2048]{2,1,0:T(8,128)(2,1)}, u32[]{:S(2)}) copy-start(bf16[1,256,2048]{2,1,0:T(8,128)(2,1)} %down_ref.3) | copy-start | bytes 3145732
  92.5 0.7 copy-start.3
  93.2 0.6 copy-start.5
  106.7 3.5 %collective-permute-start = (bf16[256,512]{1,0:T(8,128)(2,1)S(1)}, bf16[256,512]{1,0:T(8,128)(2,1)S(1)}, u32[]{:S(2)}, u32[]{:S(2)}) collective-permute-start(bf16[256,512]{1,0:T(8,128)(2,1)S(1)} %get-tuple-element.16), channel_id=1, source_target_pairs={{0,1},{1,0},{2,3},{3,2},{4,5},{5,4},{6,7},{7,6},{8,9},{9,8},{10,11... | collective-permute-start | bytes 786440 | tf_op jit(solution)/shard_map/pair/ppermute | solution.py:257
  110.2 20.6 %copy-start.6 = (bf16[2,128,128]{2,1,0:T(8,128)(2,1)S(1)}, bf16[2,128,128]{2,1,0:T(8,128)(2,1)}, u32[]{:S(2)}) copy-start(bf16[2,128,128]{2,1,0:T(8,128)(2,1)} %copy-done.5) | copy-start | bytes 196612
  110.2 20.6 %copy-start.4 = (f32[64,1024]{1,0:T(8,128)S(1)}, f32[64,1024]{1,0:T(8,128)}, u32[]{:S(2)}) copy-start(f32[64,1024]{1,0:T(8,128)} %copy-done.3) | copy-start | bytes 786436
